TPU v7x, 32 devices: a whole 2x2x4 slice. The times are simulated.
32 devices in a mesh: fs: 8 (over z, x), tp: 4 (over y, core).
Axes of the slice: x: 2, y: 2, z: 4, core: 2. Of those that a mesh axis runs over, the one named last changes fastest.
Arguments:
- later_input: bfloat16 [6144, 2048], P('fs', 'tp'), may hold values from -6 to 6
- earlier_input: bfloat16 [6144, 2048], P('fs', 'tp'), may hold values from -6 to 6
- cotangent: bfloat16 [6144, 2048], P('fs', 'tp'), may hold values from -6 to 6
- up_weight: bfloat16 [2048, 8192], P('fs', 'tp'), may hold values from -0.125 to 0.125
- down_weight: bfloat16 [8192, 2048], P('tp', 'fs'), may hold values from -0.0625 to 0.0625
- up_running: float32 [2048, 8192], P('fs', 'tp'), may hold values from -6 to 6
- down_running: float32 [2048, 8192], P('fs', 'tp'), may hold values from -6 to 6
Outputs:
- later_output: bfloat16 [6144, 2048], P('fs', 'tp')
- later_preact: bfloat16 [6144, 8192], P('fs', 'tp')
- earlier_grad: bfloat16 [6144, 2048], P('fs', 'tp')
- up_running_out: float32 [2048, 8192], P('fs', 'tp')
- down_running_out: float32 [2048, 8192], P('fs', 'tp')
All inputs are finite; a program needn't handle non-finite values.
Results may differ from a plain program's by a relative error of at most 0.014.
Values may be sent and summed in bfloat16 or wider, within the bound.
A program may use at most 128 MiB of HBM per device.

v0:
```python
import jax
import jax.numpy as jnp
from jax import lax
from jax.sharding import PartitionSpec as P

contract_last = (((1,), (1,)), ((), ()))
contract_first = (((0,), (0,)), ((), ()))


def on_device(
    later_input, earlier_input, cotangent, up_weight, down_weight, up_running, down_running
):
    rows = later_input.shape[0]
    factor = float(rows * lax.axis_size("fs")) ** (-0.5)
    later_full, earlier_full, cot_full = (
        lax.all_gather(later_input, "tp", axis=1, tiled=True),
        lax.all_gather(earlier_input, "tp", axis=1, tiled=True),
        lax.all_gather(cotangent, "tp", axis=1, tiled=True),
    )
    columns = up_weight.shape[1]
    piece = lax.all_gather(up_weight, "fs", axis=0, tiled=True)
    later_up = jnp.dot(later_full, piece, preferred_element_type=jnp.float32)
    earlier_up = jnp.dot(earlier_full, piece, preferred_element_type=jnp.float32)
    later_hidden = jnp.square(jax.nn.relu(later_up)).astype(jnp.bfloat16)
    piece = lax.all_gather(down_weight, "fs", axis=1, tiled=True)
    product = jnp.dot(later_hidden, piece, preferred_element_type=jnp.float32)
    grad = jnp.dot(cot_full, piece.T, preferred_element_type=jnp.float32)
    up_grad = (2.0 * jax.nn.relu(earlier_up) * grad).astype(jnp.bfloat16)
    back_part = lax.dot_general(
        up_grad,
        lax.all_gather(up_weight, "fs", axis=0, tiled=True),
        contract_last,
        preferred_element_type=jnp.float32,
    )
    later_preact = later_up.astype(jnp.bfloat16)
    earlier_hidden = jnp.square(jax.nn.relu(earlier_up)).astype(jnp.bfloat16)
    out_sum, back_sum = (
        lax.psum_scatter(
            product.astype(jnp.bfloat16), "tp", scatter_dimension=1, tiled=True
        ).astype(jnp.float32),
        lax.psum_scatter(
            back_part.astype(jnp.bfloat16), "tp", scatter_dimension=1, tiled=True
        ).astype(jnp.float32),
    )
    summed = lax.psum_scatter(
        jnp.concatenate(
            (
                lax.dot_general(
                    earlier_full, up_grad, contract_first, preferred_element_type=jnp.float32
                ),
                lax.dot_general(
                    cot_full, earlier_hidden, contract_first, preferred_element_type=jnp.float32
                ),
            ),
            axis=1,
        ).astype(jnp.bfloat16),
        "fs",
        scatter_dimension=0,
        tiled=True,
    ).astype(jnp.float32)
    grad_up_sum = summed[:, :columns]
    grad_down_sum = summed[:, columns:]
    return (
        out_sum.astype(jnp.bfloat16),
        later_preact,
        back_sum.astype(jnp.bfloat16),
        up_running + grad_up_sum * factor,
        down_running + grad_down_sum * factor,
    )


def solution(mesh):
    in_specs = (
        P("fs", "tp"),
        P("fs", "tp"),
        P("fs", "tp"),
        P("fs", "tp"),
        P("tp", "fs"),
        P("fs", "tp"),
        P("fs", "tp"),
    )
    out_specs = (P("fs", "tp"), P("fs", "tp"), P("fs", "tp"), P("fs", "tp"), P("fs", "tp"))
    return jax.shard_map(
        on_device, mesh=mesh, in_specs=in_specs, out_specs=out_specs, check_vma=False
    )
```

profile of v0, /device:TPU:0, one launch (start us, length us, event | category | flops | bytes accessed | tf_op | source)
XLA Modules:
  0.0 725.1 jit_solution(515259294564555302)
XLA Ops:
  7.2 0.0 all-gather.12.cloned.1.call-start
  7.2 0.7 all-gather.12.cloned.1.call-update
  7.9 0.0 all-gather.8.cloned.1.call-start
  7.9 0.7 all-gather.8.cloned.1.call-update
  8.6 0.0 all-gather.14.cloned.1.call-start
  8.7 0.7 all-gather.14.cloned.1.call-update
  9.4 0.0 all-gather.10.cloned.1.call-start
  9.4 0.5 all-gather.10.cloned.1.call-update
  10.0 0.0 all-gather.6.cloned.1.call-start
  10.0 0.5 all-gather.6.cloned.1.call-update
  10.5 0.0 reduce-scatter.8.cloned.1.call-start
  10.6 30.2 %all-gather.12.cloned.1.call-done = bf16[768,2048]{1,0:T(8,128)(2,1)} async-done(((bf16[768,512]{1,0:T(8,128)(2,1)}), bf16[768,2048]{1,0:T(8,128)(2,1)}) %all-gather.12.cloned.1.call-update) | async-done | bytes 3145744 | tf_op jit(solution)/shard_map/all_gather | solution.py:17
  40.8 126.6 %all-gather.8.cloned.1.call-done = bf16[2048,2048]{1,0:T(8,128)(2,1)} async-done(((bf16[256,2048]{1,0:T(8,128)(2,1)}), bf16[2048,2048]{1,0:T(8,128)(2,1)}) %all-gather.8.cloned.1.call-update) | async-done | bytes 8388624 | tf_op jit(solution)/shard_map/all_gather | solution.py:21
  167.4 11.6 %fusion.7 = f32[768,2048]{1,0:T(8,128)} fusion(bf16[768,2048]{1,0:T(8,128)(2,1)} %all-gather.12.cloned.1.call-done, bf16[2048,2048]{1,0:T(8,128)(2,1)} %all-gather.8.cloned.1.call-done), kind=kOutput, calls=%fused_computation.17 | convolution fusion | flops 6442450944 | bytes 17825792 | tf_op jit(solution)/shard_map/dot_general | solution.py:23
  179.1 0.0 copy-start.2
  179.1 16.6 %all-gather.14.cloned.1.call-done = bf16[768,2048]{1,0:T(8,128)(2,1)} async-done(((bf16[768,512]{1,0:T(8,128)(2,1)}), bf16[768,2048]{1,0:T(8,128)(2,1)}) %all-gather.14.cloned.1.call-update) | async-done | bytes 3145744 | tf_op jit(solution)/shard_map/all_gather | solution.py:18
  195.7 126.9 %all-gather.10.cloned.1.call-done = bf16[2048,2048]{1,0:T(8,128)(2,1)} async-done(((bf16[2048,256]{1,0:T(8,128)(2,1)}), bf16[2048,2048]{1,0:T(8,128)(2,1)}) %all-gather.10.cloned.1.call-update) | async-done | bytes 8388624 | tf_op jit(solution)/shard_map/all_gather | solution.py:25
  322.6 11.8 %multiply_convert_fusion.1 = bf16[768,2048]{1,0:T(8,128)(2,1)S(1)} fusion(f32[768,2048]{1,0:T(8,128)} %fusion.7, bf16[768,2048]{1,0:T(8,128)(2,1)} %all-gather.14.cloned.1.call-done, bf16[2048,2048]{1,0:T(8,128)(2,1)} %all-gather.10.cloned.1.call-done), kind=kOutput, calls=%fused_computation.4 | convolution fusion | flops 6448742400 | bytes 20971520 | tf_op jit(solution)/shard_map/dot_general | solution.py:27
  334.4 0.0 copy-done.2
  334.4 0.0 copy-start.4
  334.4 0.0 copy-start.3
  334.4 7.0 convert_bitcast_fusion.1
  341.4 0.0 copy-done.4
  341.4 0.0 copy-done.3
  341.4 10.0 %convert_bitcast_fusion = bf16[2048,2048]{0,1:T(8,128)(2,1)S(1)} fusion(bf16[768,2048]{1,0:T(8,128)(2,1)S(1)} %copy-done.3, f32[768,2048]{1,0:T(8,128)} %fusion.7), kind=kOutput, calls=%fused_computation.1 | convolution fusion | flops 6451363840 | bytes 17825792 | tf_op jit(solution)/shard_map/dot_general | solution.py:51
  351.4 7.5 %pad_maximum_fusion = bf16[2048,4096]{0,1:T(8,128)(2,1)} fusion(bf16[2048,2048]{0,1:T(8,128)(2,1)S(1)} %convert_bitcast_fusion, bf16[2048,2048]{0,1:T(8,128)(2,1)S(1)} %convert_bitcast_fusion.1), kind=kLoop, calls=%fused_computation | loop fusion | flops 33554432 | bytes 33554432 | tf_op jit(solution)/shard_map/concatenate | solution.py:46
  358.9 0.0 reduce-scatter.8.cloned.1.call-update
  358.9 0.0 reduce-scatter.4.cloned.1.call-start
  358.9 0.0 all-gather.6.cloned.1.call-done
  359.0 11.2 %fusion.6 = (bf16[768,2048]{1,0:T(8,128)(2,1)}, f32[768,2048]{1,0:T(8,128)S(1)}) fusion(bf16[768,2048]{1,0:T(8,128)(2,1)} %all-gather.6.cloned.1.call-done, bf16[2048,2048]{1,0:T(8,128)(2,1)} %all-gather.8.cloned.1.call-done), kind=kOutput, calls=%fused_computation.16 | convolution fusion | flops 6444023808 | bytes 20971520 | tf_op jit(solution)/shard_map/dot_general | solution.py:22
  370.1 0.0 copy-start.5
  370.1 10.4 %convolution_convert_fusion.1 = bf16[768,2048]{1,0:T(8,128)(2,1)} fusion(bf16[2048,2048]{1,0:T(8,128)(2,1)} %all-gather.10.cloned.1.call-done, f32[768,2048]{1,0:T(8,128)S(1)} %get-tuple-element.13), kind=kOutput, calls=%fused_computation.7 | convolution fusion | flops 6448742400 | bytes 17825792 | tf_op jit(solution)/shard_map/dot_general | solution.py:26
  380.6 0.0 reduce-scatter.4.cloned.1.call-update
  380.6 0.0 reduce-scatter.6.cloned.1.call-start
  380.6 0.0 copy-done.5
  380.6 10.5 %convolution_convert_fusion = bf16[768,2048]{1,0:T(8,128)(2,1)} fusion(bf16[768,2048]{1,0:T(8,128)(2,1)S(1)} %copy-done.5, bf16[2048,2048]{1,0:T(8,128)(2,1)} %all-gather.8.cloned.1.call-done), kind=kOutput, calls=%fused_computation.6 | convolution fusion | flops 6444023808 | bytes 14680064 | tf_op jit(solution)/shard_map/dot_general | solution.py:29
  391.2 0.0 reduce-scatter.6.cloned.1.call-update
  391.2 1.9 copy.13
  393.1 2.9 copy.12
  396.0 241.4 %reduce-scatter.8.cloned.1.call-done = bf16[256,4096]{0,1:T(8,128)(2,1)} async-done(((bf16[2048,4096]{0,1:T(8,128)(2,1)}), bf16[256,4096]{0,1:T(8,128)(2,1)}) %reduce-scatter.8.cloned.1.call-update) | async-done | bytes 2097168 | tf_op jit(solution)/shard_map/reduce_scatter | solution.py:45
  637.4 2.1 convert_element_type.32
  639.5 0.1 copy-done
  639.6 2.8 fusion.2
  642.4 3.0 copy.14
  645.5 0.0 copy-done.1
  645.5 1.8 copy.15
  647.3 30.1 %reduce-scatter.4.cloned.1.call-done = bf16[768,512]{1,0:T(8,128)(2,1)} async-done(((bf16[768,2048]{1,0:T(8,128)(2,1)}), bf16[768,512]{1,0:T(8,128)(2,1)}) %reduce-scatter.4.cloned.1.call-update) | async-done | bytes 786448 | tf_op jit(solution)/shard_map/reduce_scatter | solution.py:38
  677.4 40.9 %reduce-scatter.6.cloned.1.call-done = bf16[768,512]{1,0:T(8,128)(2,1)} async-done(((bf16[768,2048]{1,0:T(8,128)(2,1)}), bf16[768,512]{1,0:T(8,128)(2,1)}) %reduce-scatter.6.cloned.1.call-update) | async-done | bytes 786448 | tf_op jit(solution)/shard_map/reduce_scatter | solution.py:41
  (2 shorter events, 0.0 us)
Async XLA Ops:
  7.2 33.6 %all-gather.12.cloned.1.call-start = ((), (), s32[]{:S(2)}) async-start(), calls=%async_computation.7 | async-start | bytes 3932160 | tf_op jit(solution)/shard_map/all_gather | solution.py:17
  7.9 159.5 %all-gather.8.cloned.1.call-start = ((), (), s32[]{:S(2)}) async-start(), calls=%async_computation.4 | async-start | bytes 9437184 | tf_op jit(solution)/shard_map/all_gather | solution.py:21
  8.6 187.1 %all-gather.14.cloned.1.call-start = ((), (), s32[]{:S(2)}) async-start(), calls=%async_computation.8 | async-start | bytes 3932160 | tf_op jit(solution)/shard_map/all_gather | solution.py:18
  9.4 313.2 %all-gather.10.cloned.1.call-start = ((), (), s32[]{:S(2)}) async-start(), calls=%async_computation.5 | async-start | bytes 9437184 | tf_op jit(solution)/shard_map/all_gather | solution.py:25
  10.0 349.0 %all-gather.6.cloned.1.call-start = ((), (), s32[]{:S(2)}) async-start(), calls=%async_computation.3 | async-start | bytes 3932160 | tf_op jit(solution)/shard_map/all_gather | solution.py:16
  10.5 626.9 %reduce-scatter.8.cloned.1.call-start = ((), (), s32[]{:S(2)}) async-start(), calls=%async_computation.10 | async-start | bytes 18874368 | tf_op jit(solution)/shard_map/reduce_scatter | solution.py:45
  179.1 155.3 %copy-start.2 = (bf16[768,2048]{1,0:T(8,128)(2,1)S(1)}, bf16[768,2048]{1,0:T(8,128)(2,1)}, u32[]{:S(2)}) copy-start(bf16[768,2048]{1,0:T(8,128)(2,1)} %all-gather.12.cloned.1.call-done) | copy-start | bytes 9437188
  334.4 7.0 copy-start.4
  334.4 7.0 copy-start.3
  358.9 318.5 %reduce-scatter.4.cloned.1.call-start = ((), (), s32[]{:S(2)}) async-start(), calls=%async_computation.6 | async-start | bytes 3932160 | tf_op jit(solution)/shard_map/reduce_scatter | solution.py:38
  370.1 10.5 %copy-start.5 = (bf16[768,2048]{1,0:T(8,128)(2,1)S(1)}, bf16[768,2048]{1,0:T(8,128)(2,1)}, u32[]{:S(2)}) copy-start(bf16[768,2048]{1,0:T(8,128)(2,1)} %copy-done.4) | copy-start | bytes 9437188
  380.6 337.6 %reduce-scatter.6.cloned.1.call-start = ((), (), s32[]{:S(2)}) async-start(), calls=%async_computation.9 | async-start | bytes 3932160 | tf_op jit(solution)/shard_map/reduce_scatter | solution.py:41
  637.4 2.2 copy-start
  642.4 3.0 copy-start.1
Sparse Core Ops, SparseCore 0:
  9.5 31.2 all-gather.11
  42.9 124.4 all-gather.7
  169.0 26.6 all-gather.13
  197.6 124.9 all-gather.9
  324.0 26.6 all-gather.5
  359.0 278.3 reduce-scatter.7
  640.5 36.8 reduce-scatter.3
  680.5 37.7 reduce-scatter.5
where the time goes:
time: 725 us
  waiting for transfers between devices  616 us (85%)
  matrix products  72.5 us (10%)
  between operations  14.2 us (2%)
  other arithmetic  12.3 us (2%)
  local copies, waits for them, and re-layouts  9.82 us (1%)
    reduce_scatter x1, waiting for transfers between devices, on_device(): lax.psum_scatter(jnp.concatenate((lax.dot_general(earlier_full, up_grad,...  241 us
    all_gather x1, waiting for transfers between devices, on_device(): piece = lax.all_gather(down_weight, 'fs', axis=1, tiled=True)  127 us
    all_gather x1, waiting for transfers between devices, on_device(): piece = lax.all_gather(up_weight, 'fs', axis=0, tiled=True)  127 us
    reduce_scatter x1, waiting for transfers between devices, on_device(): lax.psum_scatter(back_part.astype(jnp.bfloat16), 'tp', scatter_dimension=...  40.9 us
    all_gather x1, waiting for transfers between devices, on_device(): lax.all_gather(earlier_input, 'tp', axis=1, tiled=True)  30.2 us
    reduce_scatter x1, waiting for transfers between devices, on_device(): lax.psum_scatter(product.astype(jnp.bfloat16), 'tp', scatter_dimension=1,...  30.1 us
    all_gather x1, waiting for transfers between devices, on_device(): lax.all_gather(cotangent, 'tp', axis=1, tiled=True)  16.6 us
  transfers between devices with their start and end apart: 8, of which 7 were waited for; matrix products, arithmetic and copies ran while one was open for 13% of the time, Pallas kernels for 0%

commit v1 on v0

--- a/solution.py
+++ b/solution.py
@@ -18,7 +18,9 @@
         lax.all_gather(cotangent, "tp", axis=1, tiled=True),
     )
     columns = up_weight.shape[1]
-    piece = lax.all_gather(up_weight, "fs", axis=0, tiled=True)
+    piece = jnp.concatenate(
+        lax.all_to_all(jnp.stack([up_weight] * lax.axis_size("fs")), "fs", 0, 0), axis=0
+    )
     later_up = jnp.dot(later_full, piece, preferred_element_type=jnp.float32)
     earlier_up = jnp.dot(earlier_full, piece, preferred_element_type=jnp.float32)
     later_hidden = jnp.square(jax.nn.relu(later_up)).astype(jnp.bfloat16)

time: 725 us -> 832 us (1.15)
  waiting for transfers between devices: 616 us -> 708 us
    all_to_all x0 -> x1, waiting for transfers between devices: none -> 260 us  [on_device(): lax.all_to_all(jnp.stack([up_weight] * lax.axis_size('fs')), 'fs', 0, 0)]
    all_gather x1, waiting for transfers between devices: 127 us -> 0.01 us  [on_device(): piece = lax.all_gather(down_weight, 'fs', axis=1, tiled=True)]
    all_gather x1, waiting for transfers between devices: 127 us -> 90.2 us  [on_device(): lax.all_gather(up_weight, 'fs', axis=0, tiled=True)]
    reduce_scatter x1, waiting for transfers between devices: 241 us -> 267 us  [on_device(): lax.psum_scatter(jnp.concatenate((lax.dot_general(earlier_full, up_grad,...]
    all_gather x1, waiting for transfers between devices: 16.6 us -> 0.01 us  [on_device(): lax.all_gather(cotangent, 'tp', axis=1, tiled=True)]
    all_gather x1, waiting for transfers between devices: 30.2 us -> 17.4 us  [on_device(): lax.all_gather(earlier_input, 'tp', axis=1, tiled=True)]
  transfers between devices with their start and end apart: 8 -> 9, of which waited for: 7 -> 6; matrix products, arithmetic and copies ran while one was open for 13% -> 12% of each run, Pallas kernels for 0% -> 0%
where the time goes in v1:
time: 832 us
  waiting for transfers between devices  708 us (85%)
  matrix products  73.3 us (9%)
  local copies, waits for them, and re-layouts  16.3 us (2%)
  between operations  14.2 us (2%)
  other arithmetic  12.2 us (1%)
    reduce_scatter x1, waiting for transfers between devices, on_device(): lax.psum_scatter(jnp.concatenate((lax.dot_general(earlier_full, up_grad,...  267 us
    all_to_all x1, waiting for transfers between devices, on_device(): lax.all_to_all(jnp.stack([up_weight] * lax.axis_size('fs')), 'fs', 0, 0)  260 us
    all_gather x1, waiting for transfers between devices, on_device(): lax.all_gather(up_weight, 'fs', axis=0, tiled=True)  90.2 us
    reduce_scatter x1, waiting for transfers between devices, on_device(): lax.psum_scatter(back_part.astype(jnp.bfloat16), 'tp', scatter_dimension=...  40.9 us
    reduce_scatter x1, waiting for transfers between devices, on_device(): lax.psum_scatter(product.astype(jnp.bfloat16), 'tp', scatter_dimension=1,...  29.3 us
    all_gather x1, waiting for transfers between devices, on_device(): lax.all_gather(earlier_input, 'tp', axis=1, tiled=True)  17.4 us
  transfers between devices with their start and end apart: 9, of which 6 were waited for; matrix products, arithmetic and copies ran while one was open for 12% of the time, Pallas kernels for 0%

profile of v1, /device:TPU:0, one launch (start us, length us, event | category | flops | bytes accessed | tf_op | source)
XLA Modules:
  0.0 832.0 jit_solution(9401762031708735880)
XLA Ops:
  7.2 0.0 all-gather.10.cloned.1.call-start
  7.2 0.7 all-gather.10.cloned.1.call-update
  7.9 0.0 all-gather.12.cloned.1.call-start
  7.9 0.7 all-gather.12.cloned.1.call-update
  8.6 0.0 all-gather.8.cloned.1.call-start
  8.7 0.7 all-gather.8.cloned.1.call-update
  9.4 5.5 stack.2
  14.9 7.3 all-to-all-start
  22.2 0.0 all-gather.6.cloned.1.call-start
  22.3 0.5 all-gather.6.cloned.1.call-update
  22.8 0.0 all-gather.14.cloned.1.call-start
  22.8 0.5 all-gather.14.cloned.1.call-update
  23.4 0.0 reduce-scatter.8.cloned.1.call-start
  23.4 17.4 %all-gather.10.cloned.1.call-done = bf16[768,2048]{1,0:T(8,128)(2,1)} async-done(((bf16[768,512]{1,0:T(8,128)(2,1)}), bf16[768,2048]{1,0:T(8,128)(2,1)}) %all-gather.10.cloned.1.call-update) | async-done | bytes 3145744 | tf_op jit(solution)/shard_map/all_gather | solution.py:17
  40.8 260.4 %all-to-all-done = bf16[8,256,2048]{2,1,0:T(8,128)(2,1)} async-done(((bf16[8,256,2048]{2,1,0:T(8,128)(2,1)}), bf16[8,256,2048]{2,1,0:T(8,128)(2,1)}, u32[]{:S(2)}, u32[]{:S(2)}) %all-to-all-start) | async-done | bytes 8388640 | tf_op jit(solution)/shard_map/all_to_all | solution.py:22
  301.2 11.7 %fusion.7 = f32[768,2048]{1,0:T(8,128)} fusion(bf16[768,2048]{1,0:T(8,128)(2,1)} %all-gather.10.cloned.1.call-done, bf16[2048,2048]{1,0:T(8,128)(2,1)} %bitcast), kind=kOutput, calls=%fused_computation.17 | convolution fusion | flops 6442450944 | bytes 17825792 | tf_op jit(solution)/shard_map/dot_general | solution.py:25
  312.9 0.0 copy-start.1
  312.9 0.0 all-gather.12.cloned.1.call-done
  312.9 12.8 %multiply_convert_fusion.1 = bf16[768,2048]{1,0:T(8,128)(2,1)S(1)} fusion(f32[768,2048]{1,0:T(8,128)} %fusion.7, bf16[768,2048]{1,0:T(8,128)(2,1)} %all-gather.12.cloned.1.call-done, bf16[2048,2048]{1,0:T(8,128)(2,1)} %all-gather.8.cloned.1.call-done), kind=kOutput, calls=%fused_computation.4 | convolution fusion | flops 6448742400 | bytes 20971520 | tf_op jit(solution)/shard_map/dot_general | solution.py:29
  325.7 0.0 copy-done.1
  325.7 0.0 copy-start.3
  325.7 0.0 copy-start.2
  325.7 7.0 convert_bitcast_fusion.1
  332.7 0.0 copy-done.3
  332.7 0.0 copy-done.2
  332.7 10.0 %convert_bitcast_fusion = bf16[2048,2048]{0,1:T(8,128)(2,1)S(1)} fusion(bf16[768,2048]{1,0:T(8,128)(2,1)S(1)} %copy-done.2, f32[768,2048]{1,0:T(8,128)} %fusion.7), kind=kOutput, calls=%fused_computation.1 | convolution fusion | flops 6451363840 | bytes 17825792 | tf_op jit(solution)/shard_map/dot_general | solution.py:53
  342.7 7.5 pad_maximum_fusion
  350.2 0.0 reduce-scatter.8.cloned.1.call-update
  350.3 0.0 reduce-scatter.4.cloned.1.call-start
  350.3 0.0 all-gather.6.cloned.1.call-done
  350.3 11.2 %fusion.6 = (bf16[768,2048]{1,0:T(8,128)(2,1)}, f32[768,2048]{1,0:T(8,128)S(1)}) fusion(bf16[768,2048]{1,0:T(8,128)(2,1)} %all-gather.6.cloned.1.call-done, bf16[2048,2048]{1,0:T(8,128)(2,1)} %bitcast), kind=kOutput, calls=%fused_computation.16 | convolution fusion | flops 6444023808 | bytes 20971520 | tf_op jit(solution)/shard_map/dot_general | solution.py:24
  361.5 10.4 %convolution_convert_fusion.1 = bf16[768,2048]{1,0:T(8,128)(2,1)} fusion(bf16[2048,2048]{1,0:T(8,128)(2,1)} %all-gather.8.cloned.1.call-done, f32[768,2048]{1,0:T(8,128)S(1)} %get-tuple-element.13), kind=kOutput, calls=%fused_computation.7 | convolution fusion | flops 6448742400 | bytes 17825792 | tf_op jit(solution)/shard_map/dot_general | solution.py:28
  371.9 0.0 reduce-scatter.4.cloned.1.call-update
  372.0 0.0 reduce-scatter.6.cloned.1.call-start
  372.0 90.2 %all-gather.14.cloned.1.call-done = bf16[2048,2048]{1,0:T(8,128)(2,1)} async-done(((bf16[256,2048]{1,0:T(8,128)(2,1)}), bf16[2048,2048]{1,0:T(8,128)(2,1)}) %all-gather.14.cloned.1.call-update) | async-done | bytes 8388624 | tf_op jit(solution)/shard_map/all_gather | solution.py:33
  462.3 0.0 copy-done.4
  462.3 10.3 %convolution_convert_fusion = bf16[768,2048]{1,0:T(8,128)(2,1)} fusion(bf16[768,2048]{1,0:T(8,128)(2,1)S(1)} %copy-done.4, bf16[2048,2048]{1,0:T(8,128)(2,1)} %all-gather.14.cloned.1.call-done), kind=kOutput, calls=%fused_computation.6 | convolution fusion | flops 6444023808 | bytes 14680064 | tf_op jit(solution)/shard_map/dot_general | solution.py:31
  472.5 0.0 reduce-scatter.6.cloned.1.call-update
  472.5 1.9 copy.13
  474.5 2.9 copy.12
  477.4 267.0 %reduce-scatter.8.cloned.1.call-done = bf16[256,4096]{0,1:T(8,128)(2,1)} async-done(((bf16[2048,4096]{0,1:T(8,128)(2,1)}), bf16[256,4096]{0,1:T(8,128)(2,1)}) %reduce-scatter.8.cloned.1.call-update) | async-done | bytes 2097168 | tf_op jit(solution)/shard_map/reduce_scatter | solution.py:47
  744.4 2.1 convert_element_type.32
  746.4 0.1 copy-done
  746.6 2.7 fusion.2
  749.3 2.9 copy.14
  752.1 2.9 copy.15
  755.0 29.3 %reduce-scatter.4.cloned.1.call-done = bf16[768,512]{1,0:T(8,128)(2,1)} async-done(((bf16[768,2048]{1,0:T(8,128)(2,1)}), bf16[768,512]{1,0:T(8,128)(2,1)}) %reduce-scatter.4.cloned.1.call-update) | async-done | bytes 786448 | tf_op jit(solution)/shard_map/reduce_scatter | solution.py:40
  784.3 40.9 %reduce-scatter.6.cloned.1.call-done = bf16[768,512]{1,0:T(8,128)(2,1)} async-done(((bf16[768,2048]{1,0:T(8,128)(2,1)}), bf16[768,512]{1,0:T(8,128)(2,1)}) %reduce-scatter.6.cloned.1.call-update) | async-done | bytes 786448 | tf_op jit(solution)/shard_map/reduce_scatter | solution.py:43
  (3 shorter events, 0.0 us)
Async XLA Ops:
  7.2 33.6 %all-gather.10.cloned.1.call-start = ((), (), s32[]{:S(2)}) async-start(), calls=%async_computation.7 | async-start | bytes 3932160 | tf_op jit(solution)/shard_map/all_gather | solution.py:17
  7.9 305.0 %all-gather.12.cloned.1.call-start = ((), (), s32[]{:S(2)}) async-start(), calls=%async_computation.8 | async-start | bytes 3932160 | tf_op jit(solution)/shard_map/all_gather | solution.py:18
  8.6 304.3 %all-gather.8.cloned.1.call-start = ((), (), s32[]{:S(2)}) async-start(), calls=%async_computation.5 | async-start | bytes 9437184 | tf_op jit(solution)/shard_map/all_gather | solution.py:27
  14.9 286.2 %all-to-all-start = ((bf16[8,256,2048]{2,1,0:T(8,128)(2,1)}), bf16[8,256,2048]{2,1,0:T(8,128)(2,1)}, u32[]{:S(2)}, u32[]{:S(2)}) async-start(bf16[8,256,2048]{2,1,0:T(8,128)(2,1)} %stack.2), calls=%async_computation | async-start | bytes 16777216 | tf_op jit(solution)/shard_map/all_to_all | solution.py:22
  22.2 328.1 %all-gather.6.cloned.1.call-start = ((), (), s32[]{:S(2)}) async-start(), calls=%async_computation.4 | async-start | bytes 3932160 | tf_op jit(solution)/shard_map/all_gather | solution.py:16
  22.8 439.5 %all-gather.14.cloned.1.call-start = ((), (), s32[]{:S(2)}) async-start(), calls=%async_computation.9 | async-start | bytes 9437184 | tf_op jit(solution)/shard_map/all_gather | solution.py:33
  23.4 721.0 %reduce-scatter.8.cloned.1.call-start = ((), (), s32[]{:S(2)}) async-start(), calls=%async_computation.11 | async-start | bytes 18874368 | tf_op jit(solution)/shard_map/reduce_scatter | solution.py:47
  312.9 12.8 %copy-start.1 = (bf16[768,2048]{1,0:T(8,128)(2,1)S(1)}, bf16[768,2048]{1,0:T(8,128)(2,1)}, u32[]{:S(2)}) copy-start(bf16[768,2048]{1,0:T(8,128)(2,1)} %all-gather.10.cloned.1.call-done) | copy-start | bytes 9437188
  325.7 7.0 copy-start.3
  325.7 7.0 copy-start.2
  350.3 434.1 %reduce-scatter.4.cloned.1.call-start = ((), (), s32[]{:S(2)}) async-start(), calls=%async_computation.6 | async-start | bytes 3932160 | tf_op jit(solution)/shard_map/reduce_scatter | solution.py:40
  361.5 100.7 %copy-start.4 = (bf16[768,2048]{1,0:T(8,128)(2,1)S(1)}, bf16[768,2048]{1,0:T(8,128)(2,1)}, u32[]{:S(2)}) copy-start(bf16[768,2048]{1,0:T(8,128)(2,1)} %copy-done.3) | copy-start | bytes 9437188
  372.0 453.2 %reduce-scatter.6.cloned.1.call-start = ((), (), s32[]{:S(2)}) async-start(), calls=%async_computation.10 | async-start | bytes 3932160 | tf_op jit(solution)/shard_map/reduce_scatter | solution.py:43
  744.4 2.2 copy-start
Sparse Core Ops, SparseCore 0:
  9.5 31.2 all-gather.9
  42.4 28.4 all-gather.11
  73.0 233.8 all-gather.7
  308.2 27.4 all-gather.5
  337.8 124.4 all-gather.13
  465.9 278.4 reduce-scatter.7
  747.5 36.8 reduce-scatter.3
  787.4 37.7 reduce-scatter.5
